TPU v7x, 32 devices: a whole 2x2x4 slice. The times are simulated.
32 devices in a mesh: fs: 8 (over z, x), tp: 4 (over y, core).
Axes of the slice: x: 2, y: 2, z: 4, core: 2. Of those that a mesh axis runs over, the one named last changes fastest.
Arguments:
- normed_input: bfloat16 [8192, 2048], P('fs'), may hold values from -64 to 64
- query_cotangent: bfloat16 [8192, 1024], P('fs', 'tp'), may hold values from -6 to 6
- key_cotangent: bfloat16 [8192, 512], P('fs', 'tp'), may hold values from -6 to 6
- query_weight: float32 [2048, 1024], P('fs', 'tp'), may hold values from -6 to 6
- key_weight: float32 [2048, 512], P('fs', 'tp'), may hold values from -6 to 6
- query_basis: bfloat16 [1024, 128], P('tp'), may hold values from -1 to 1
- key_basis: bfloat16 [512, 128], P('tp'), may hold values from -1 to 1
- moment_mean: float32 [2, 2048, 128], P(None, 'fs'), may hold values from -3 to 3
- moment_square: float32 [2, 2048, 128], P(None, 'fs'), may hold values from 0.25 to 4
Outputs:
- query_step: float32 [2048, 1024], P('fs', 'tp')
- key_step: float32 [2048, 512], P('fs', 'tp')
- query_updated: float32 [2048, 1024], P('fs', 'tp')
- key_updated: float32 [2048, 512], P('fs', 'tp')
- query_copy: bfloat16 [2048, 1024], P('fs', 'tp')
- key_copy: bfloat16 [2048, 512], P('fs', 'tp')
- mean_updated: float32 [2, 2048, 128], P(None, 'fs')
- square_updated: float32 [2, 2048, 128], P(None, 'fs')
All inputs are finite; a program needn't handle non-finite values.
Results may differ from a plain program's by a relative error of at most 0.0011.
Values sent between devices are 32-bit elements; how exact they have to be, the bound alone decides.
A program may use at most 64 MiB of HBM per device.

v0:
```python
import jax
import jax.numpy as jnp
from jax import lax
from jax.sharding import PartitionSpec as P

BETA_MEAN = 0.75
BETA_SQUARE = 0.8
STEP_RATE = 0.25
EPSILON = 1e-06


def local(
    normed_input,
    query_cotangent,
    key_cotangent,
    query_weight,
    key_weight,
    query_basis,
    key_basis,
    moment_mean,
    moment_square,
):
    highest = lax.Precision.HIGHEST
    contract = (((0,), (0,)), ((), ()))
    row_count = query_weight.shape[0]
    rank_width = query_basis.shape[1]
    query_float = query_basis.astype(jnp.float32)
    key_float = key_basis.astype(jnp.float32)
    partial_precision = lax.Precision.HIGH
    query_part = lax.dot_general(
        normed_input, query_cotangent, contract, preferred_element_type=jnp.float32
    )
    key_part = lax.dot_general(
        normed_input, key_cotangent, contract, preferred_element_type=jnp.float32
    )
    query_part, key_part = (query_part, key_part)
    summed = lax.psum_scatter(
        jnp.concatenate(
            [
                jnp.dot(query_part, query_float, precision=partial_precision),
                jnp.dot(key_part, key_float, precision=partial_precision),
            ],
            axis=1,
        ),
        "fs",
        scatter_dimension=0,
        tiled=True,
    )
    query_projected = summed[:, :rank_width]
    key_projected = summed[:, rank_width:]
    projected = lax.psum(jnp.stack([query_projected, key_projected]), "tp")
    total_square = lax.psum(jnp.sum(projected * projected), "fs")
    entry_count = 2.0 * row_count * lax.axis_size("fs") * rank_width
    normalized = projected * lax.rsqrt(total_square / entry_count + EPSILON)
    mean_updated = BETA_MEAN * moment_mean + (1.0 - BETA_MEAN) * normalized
    square_updated = BETA_SQUARE * moment_square + (1.0 - BETA_SQUARE) * normalized * normalized
    direction = mean_updated / jnp.sqrt(square_updated)
    outer = (((1,), (1,)), ((), ()))
    query_step = lax.dot_general(direction[0], query_float, outer, precision=highest)
    key_step = lax.dot_general(direction[1], key_float, outer, precision=highest)
    query_updated = query_weight - STEP_RATE * query_step
    key_updated = key_weight - STEP_RATE * key_step
    return (
        query_step,
        key_step,
        query_updated,
        key_updated,
        query_updated.astype(jnp.bfloat16),
        key_updated.astype(jnp.bfloat16),
        mean_updated,
        square_updated,
    )


def solution(mesh):
    in_specs = (
        P("fs", None),
        P("fs", "tp"),
        P("fs", "tp"),
        P("fs", "tp"),
        P("fs", "tp"),
        P("tp", None),
        P("tp", None),
        P(None, "fs", None),
        P(None, "fs", None),
    )
    out_specs = (
        P("fs", "tp"),
        P("fs", "tp"),
        P("fs", "tp"),
        P("fs", "tp"),
        P("fs", "tp"),
        P("fs", "tp"),
        P(None, "fs", None),
        P(None, "fs", None),
    )
    return jax.shard_map(local, mesh=mesh, in_specs=in_specs, out_specs=out_specs, check_vma=False)
```

profile of v0, /device:TPU:0, one launch (start us, length us, event | category | flops | bytes accessed | tf_op | source)
XLA Modules:
  0.0 158.6 jit_solution(541091675263221760)
XLA Ops:
  7.2 0.0 copy-start
  7.2 0.0 copy-start.2
  7.2 0.0 reduce-scatter.2.cloned.1.call-start
  7.2 1.0 copy-done
  8.2 0.0 copy-start.1
  8.2 3.7 %fusion.6 = f32[2048,256]{1,0:T(8,128)S(1)} fusion(bf16[1024,2048]{1,0:T(8,128)(2,1)} %param.9, bf16[1024,256]{1,0:T(8,128)(2,1)S(1)} %copy-done), kind=kOutput, calls=%fused_computation.17 | convolution fusion | flops 1073741824 | bytes 6815744 | tf_op jit(solution)/shard_map/dot_general | solution.py:30
  11.9 0.0 copy-done.2
  11.9 0.0 copy-done.1
  11.9 0.0 copy-start.4
  11.9 1.3 fusion.8
  13.2 0.0 copy-done.4
  13.3 0.0 copy-start.7
  13.3 0.8 fusion.7
  14.1 0.0 copy-done.7
  14.1 0.5 fusion.9
  14.6 1.5 pad_maximum_fusion
  16.1 0.0 copy-start.5
  16.1 0.0 copy-start.6
  16.1 0.0 reduce-scatter.2.cloned.1.call-update
  16.1 0.0 copy-start.3
  16.2 0.0 all-reduce.2.cloned.1.call-start
  16.2 72.0 %reduce-scatter.2.cloned.1.call-done = f32[256,256]{0,1:T(8,128)} async-done(((f32[2048,256]{0,1:T(8,128)}), f32[256,256]{0,1:T(8,128)}) %reduce-scatter.2.cloned.1.call-update) | async-done | bytes 262160 | tf_op jit(solution)/shard_map/reduce_scatter | solution.py:37
  88.2 1.0 slice_bitcast_fusion.5
  89.2 0.7 pad_maximum_fusion.1
  89.9 0.0 copy-start.8
  89.9 0.0 all-reduce.2.cloned.1.call-update
  89.9 0.0 copy-done.5
  89.9 0.1 copy.17
  90.0 32.4 %all-reduce.2.cloned.1.call-done = f32[2,256,128]{1,2,0:T(8,128)} async-done(((f32[2,256,128]{1,2,0:T(8,128)}), f32[2,256,128]{1,2,0:T(8,128)}) %all-reduce.2.cloned.1.call-update) | async-done | bytes 262160 | tf_op jit(solution)/shard_map/psum | solution.py:51
  122.4 1.6 %multiply_reduce_fusion = f32[]{:T(128)} fusion(f32[2,256,128]{1,2,0:T(8,128)} %all-reduce.2.cloned.1.call-done), kind=kLoop, calls=%fused_computation.7 | loop fusion | flops 131071 | bytes 262148 | tf_op jit(solution)/shard_map/reduce_sum | solution.py:52
  124.1 0.0 copy-done.6
  124.1 0.1 copy.18
  124.2 22.0 %psum.15 = f32[]{:T(128)} all-reduce(f32[]{:T(128)} %multiply_reduce_fusion), channel_id=1, replica_groups=mesh['fs'=8,'tp'=4] {'fs'}, use_global_device_ids=true, to_apply=%region_3.0 | all-reduce | flops 1 | bytes 8 | tf_op jit(solution)/shard_map/psum | solution.py:52
  146.9 1.0 rsqrt_multiply_fusion
  147.9 0.0 copy-done.3
  147.9 1.1 fusion.4
  149.1 0.0 copy-done.8
  149.1 1.0 fusion.3
  150.1 0.8 copy.19
  150.9 0.8 copy.20
Async XLA Ops:
  7.2 1.0 copy-start
  7.2 4.7 %copy-start.2 = (bf16[1024,128]{1,0:T(8,128)(2,1)S(1)}, bf16[1024,128]{1,0:T(8,128)(2,1)}, u32[]{:S(2)}) copy-start(bf16[1024,128]{1,0:T(8,128)(2,1)} %param.11) | copy-start | bytes 786436
  7.2 81.0 %reduce-scatter.2.cloned.1.call-start = ((), (), s32[]{:S(2)}) async-start(), calls=%async_computation.1 | async-start | bytes 2359296 | tf_op jit(solution)/shard_map/reduce_scatter | solution.py:37
  8.2 3.7 %copy-start.1 = (bf16[1024,2048]{1,0:T(8,128)(2,1)S(1)}, bf16[1024,2048]{1,0:T(8,128)(2,1)}, u32[]{:S(2)}) copy-start(bf16[1024,2048]{1,0:T(8,128)(2,1)} %param.9) | copy-start | bytes 12582916
  11.9 1.3 copy-start.4
  13.3 0.9 copy-start.7
  16.1 73.8 %copy-start.5 = (f32[2,256,128]{2,1,0:T(8,128)S(1)}, f32[2,256,128]{2,1,0:T(8,128)}, u32[]{:S(2)}) copy-start(f32[2,256,128]{2,1,0:T(8,128)} %param.16) | copy-start | bytes 786436
  16.1 107.9 %copy-start.6 = (f32[2,256,128]{2,1,0:T(8,128)S(1)}, f32[2,256,128]{2,1,0:T(8,128)}, u32[]{:S(2)}) copy-start(f32[2,256,128]{2,1,0:T(8,128)} %param.17) | copy-start | bytes 786436
  16.1 131.8 %copy-start.3 = (f32[256,256]{1,0:T(8,128)S(1)}, f32[256,256]{1,0:T(8,128)}, u32[]{:S(2)}) copy-start(f32[256,256]{1,0:T(8,128)} %param.12) | copy-start | bytes 786436
  16.2 106.3 %all-reduce.2.cloned.1.call-start = ((), (), s32[]{:S(2)}) async-start(), calls=%async_computation.2 | async-start | bytes 524288 | tf_op jit(solution)/shard_map/psum | solution.py:51
  89.9 59.2 %copy-start.8 = (f32[256,128]{1,0:T(8,128)S(1)}, f32[256,128]{1,0:T(8,128)}, u32[]{:S(2)}) copy-start(f32[256,128]{1,0:T(8,128)} %param.13) | copy-start | bytes 393220
Sparse Core Ops, SparseCore 0:
  16.3 71.8 reduce-scatter.1
  91.1 31.3 all-reduce.1
where the time goes:
time: 159 us
  waiting for transfers between devices  104 us (65%)
  blocking collectives  22 us (14%)
  between operations  14.9 us (9%)
  matrix products  8.46 us (5%)
  other arithmetic  4.88 us (3%)
  local copies, waits for them, and re-layouts  3.93 us (2%)
    reduce_scatter x1, waiting for transfers between devices, local(): lax.psum_scatter(jnp.concatenate([jnp.dot(query_part, query_float, precis...  72 us
    psum x1, waiting for transfers between devices, local(): projected = lax.psum(jnp.stack([query_projected, key_projected]), 'tp')  32.4 us
    psum x1, blocking collectives, local(): total_square = lax.psum(jnp.sum(projected * projected), 'fs')  22 us
    dot_general x1, matrix products, local(): lax.dot_general(normed_input, query_cotangent, contract, preferred_elemen...  3.68 us
  transfers between devices with their start and end apart: 2, of which 2 were waited for; matrix products, arithmetic and copies ran while one was open for 0% of the time, Pallas kernels for 0%

commit v1 on v0

v1 whole, which is shorter than its diff:
```python
import functools

import jax
import jax.numpy as jnp
from jax import lax
from jax.experimental import pallas as pl
from jax.experimental.pallas import tpu as pltpu
from jax.sharding import PartitionSpec as P

BETA_MEAN = 0.75
BETA_SQUARE = 0.8
STEP_RATE = 0.25
EPSILON = 1e-06
CHUNKS = 4
MESH = pl.DeviceIdType.MESH
NT = (((1,), (1,)), ((), ()))


def split(value):
    high = value.astype(jnp.bfloat16)
    low = (value - high.astype(jnp.float32)).astype(jnp.bfloat16)
    return high, low


def reduce_kernel(
    n_fs,
    n_tp,
    x_hbm,
    cq_hbm,
    ck_hbm,
    bq_ref,
    bk_ref,
    out_ref,
    total_ref,
    x_ref,
    cq_ref,
    ck_ref,
    ybuf,
    ycore,
    ysum,
    yrecv,
    pbuf,
    xrecv,
    qbuf,
    zrecv,
    gather,
    square,
    squares,
    load_sem,
    core_send,
    core_recv,
    y_send,
    y_recv,
    x_send,
    x_recv,
    z_send,
    z_recv,
    g_send,
    g_recv,
    s_send,
    s_recv,
):
    f = lax.axis_index("fs")
    t = lax.axis_index("tp")
    tp_outer, fs_outer = n_tp // 2, n_fs // 2
    y, core = t // 2, t % 2
    z, x = f // 2, f % 2
    chunks, depth = ybuf.shape[0], ybuf.shape[3]
    rows = pbuf.shape[-1]
    rank = bq_ref.shape[1]

    def peer(df, dt):
        return (lax.rem(f + df, n_fs), lax.rem(t + dt, n_tp))

    others = [(df, dt) for df in range(n_fs) for dt in range(n_tp) if df or dt]

    loads = [
        pltpu.make_async_copy(cq_hbm, cq_ref, load_sem.at[0]),
        pltpu.make_async_copy(ck_hbm, ck_ref, load_sem.at[1]),
        pltpu.make_async_copy(x_hbm, x_ref, load_sem.at[2]),
    ]
    for load in loads:
        load.start()
    barrier = pltpu.get_barrier_semaphore()
    for df, dt in others:
        pl.semaphore_signal(barrier, inc=1, device_id=peer(df, dt), device_id_type=MESH)

    per = chunks * depth
    for which, (basis, cot) in enumerate(((bq_ref, cq_ref), (bk_ref, ck_ref))):
        loads[which].wait()
        part = lax.dot_general(
            basis[...].T, cot[...], NT, preferred_element_type=jnp.float32
        )
        for start in range(0, rank, depth):
            owner, c = divmod(which * rank + start, per)
            ybuf[c // depth, owner % 2, owner // 2] = part[start : start + depth]

    pl.semaphore_wait(barrier, len(others))

    def remote(src, dst, send, recv, device):
        return pltpu.make_async_remote_copy(
            src_ref=src, dst_ref=dst, send_sem=send, recv_sem=recv,
            device_id=device, device_id_type=MESH,
        )

    started = []

    core_copies = []
    for c in range(chunks):
        copy = remote(
            ybuf.at[c, 1 - core], ycore.at[c], core_send.at[c], core_recv.at[c],
            (f, y * 2 + 1 - core),
        )
        copy.start()
        core_copies.append(copy)
    started += core_copies

    y_copies = {}
    x_copies = {}
    z_copies = {}
    g_copies = {}

    def stage_core(c):
        core_copies[c].wait_recv()
        for o in range(tp_outer):
            ysum[c, o] = ybuf[c, core, o] + ycore[c, o]
        for d in range(1, tp_outer):
            to = lax.rem(y + d, tp_outer)
            copy = remote(
                ysum.at[c, to], yrecv.at[c, d - 1],
                y_send.at[c, d - 1], y_recv.at[c, d - 1], (f, to * 2 + core),
            )
            copy.start()
            y_copies[c, d] = copy
            started.append(copy)

    def stage_y(c):
        value = ysum[c, y]
        for d in range(1, tp_outer):
            y_copies[c, d].wait_recv()
            value = value + yrecv[c, d - 1]
        both = jnp.concatenate(split(value), axis=0)
        if c == 0:
            loads[2].wait()
        for o in range(fs_outer):
            wide = jnp.dot(
                both, x_ref[:, o * 2 * rows : (o + 1) * 2 * rows],
                preferred_element_type=jnp.float32,
            )
            wide = wide[:depth] + wide[depth:]
            pbuf[c, 0, o] = wide[:, :rows]
            pbuf[c, 1, o] = wide[:, rows:]
        copy = remote(
            pbuf.at[c, 1 - x], xrecv.at[c], x_send.at[c], x_recv.at[c],
            (z * 2 + 1 - x, t),
        )
        copy.start()
        x_copies[c] = copy
        started.append(copy)

    def stage_x(c):
        x_copies[c].wait_recv()
        for o in range(fs_outer):
            qbuf[c, o] = pbuf[c, x, o] + xrecv[c, o]
        for d in range(1, fs_outer):
            to = lax.rem(z + d, fs_outer)
            copy = remote(
                qbuf.at[c, to], zrecv.at[c, d - 1],
                z_send.at[c, d - 1], z_recv.at[c, d - 1], (to * 2 + x, t),
            )
            copy.start()
            z_copies[c, d] = copy
            started.append(copy)

    def stage_z(c):
        value = qbuf[c, z]
        for d in range(1, fs_outer):
            z_copies[c, d].wait_recv()
            value = value + zrecv[c, d - 1]
        gather[t, c] = value
        for d in range(1, n_tp):
            copy = remote(
                gather.at[t, c], gather.at[t, c],
                g_send.at[c, d - 1], g_recv.at[c, d - 1], peer(0, d),
            )
            copy.start()
            g_copies[c, d] = copy
            started.append(copy)
        powers = value * value
        acc = None
        for i in range(0, depth, 8):
            for j in range(0, rows, 128):
                piece = powers[i : i + 8, j : j + 128]
                acc = piece if acc is None else acc + piece
        return acc

    for c in range(chunks):
        stage_core(c)
    acc = None
    for step in range(chunks + 2):
        if step < chunks:
            stage_y(step)
        if 0 <= step - 1 < chunks:
            stage_x(step - 1)
        if 0 <= step - 2 < chunks:
            piece = stage_z(step - 2)
            acc = piece if acc is None else acc + piece

    square[...] = acc
    s_copies = []
    for i, (df, dt) in enumerate(others):
        copy = remote(square, squares.at[i], s_send.at[i], s_recv.at[i], peer(df, dt))
        copy.start()
        s_copies.append(copy)
    started += s_copies
    for c in range(chunks):
        for d in range(1, n_tp):
            g_copies[c, d].wait_recv()
    for o in range(n_tp):
        for c in range(chunks):
            out_ref[(o * chunks + c) * depth : (o * chunks + c + 1) * depth, :] = gather[o, c]
    for copy in s_copies:
        copy.wait_recv()
    for i in range(len(others)):
        acc = acc + squares[i]
    total_ref[...] = acc
    for copy in started:
        copy.wait_send()


def update_kernel(
    entry_count,
    sums_ref,
    total_ref,
    qw_ref,
    kw_ref,
    bq_ref,
    bk_ref,
    mean_ref,
    sq_ref,
    qs_out,
    ks_out,
    qu_out,
    ku_out,
    qc_out,
    kc_out,
    mean_out,
    sq_out,
):
    rank = bq_ref.shape[1]
    scale = lax.rsqrt(jnp.sum(total_ref[...], keepdims=True) / entry_count + EPSILON)
    sets = (
        (bq_ref, qw_ref, qs_out, qu_out, qc_out),
        (bk_ref, kw_ref, ks_out, ku_out, kc_out),
    )
    for which, (basis, weight, step_out, new_out, copy_out) in enumerate(sets):
        normalized = sums_ref[which * rank : (which + 1) * rank, :].T * scale
        mean = BETA_MEAN * mean_ref[which] + (1.0 - BETA_MEAN) * normalized
        second = BETA_SQUARE * sq_ref[which] + (1.0 - BETA_SQUARE) * normalized * normalized
        mean_out[which] = mean
        sq_out[which] = second
        high, low = split(mean / jnp.sqrt(second))
        step = lax.dot_general(high, basis[...], NT, preferred_element_type=jnp.float32)
        step += lax.dot_general(low, basis[...], NT, preferred_element_type=jnp.float32)
        new = weight[...] - STEP_RATE * step
        step_out[...] = step
        new_out[...] = new
        copy_out[...] = new.astype(jnp.bfloat16)


def fast(n_fs, n_tp, x, cq, ck, qw, kw, bq, bk, mean, sq):
    tokens, width = x.shape
    rows = qw.shape[0]
    rank = bq.shape[1]
    depth = 2 * rank // n_tp // CHUNKS
    tp_outer, fs_outer = n_tp // 2, n_fs // 2
    f32 = jnp.float32
    k = CHUNKS
    dma = pltpu.SemaphoreType.DMA
    hbm = pl.BlockSpec(memory_space=pl.ANY)
    vmem = pl.BlockSpec(memory_space=pltpu.VMEM)
    sums, total = pl.pallas_call(
        functools.partial(reduce_kernel, n_fs, n_tp),
        out_shape=(
            jax.ShapeDtypeStruct((2 * rank, rows), f32),
            jax.ShapeDtypeStruct((8, 128), f32),
        ),
        in_specs=[hbm, hbm, hbm, vmem, vmem],
        out_specs=(vmem, vmem),
        scratch_shapes=[
            pltpu.VMEM(x.shape, x.dtype),
            pltpu.VMEM(cq.shape, cq.dtype),
            pltpu.VMEM(ck.shape, ck.dtype),
            pltpu.VMEM((k, 2, tp_outer, depth, tokens), f32),
            pltpu.VMEM((k, tp_outer, depth, tokens), f32),
            pltpu.VMEM((k, tp_outer, depth, tokens), f32),
            pltpu.VMEM((k, tp_outer - 1, depth, tokens), f32),
            pltpu.VMEM((k, 2, fs_outer, depth, rows), f32),
            pltpu.VMEM((k, fs_outer, depth, rows), f32),
            pltpu.VMEM((k, fs_outer, depth, rows), f32),
            pltpu.VMEM((k, fs_outer - 1, depth, rows), f32),
            pltpu.VMEM((n_tp, k, depth, rows), f32),
            pltpu.VMEM((8, 128), f32),
            pltpu.VMEM((n_fs * n_tp - 1, 8, 128), f32),
            dma((3,)),
            dma((k,)),
            dma((k,)),
            dma((k, tp_outer - 1)),
            dma((k, tp_outer - 1)),
            dma((k,)),
            dma((k,)),
            dma((k, fs_outer - 1)),
            dma((k, fs_outer - 1)),
            dma((k, n_tp - 1)),
            dma((k, n_tp - 1)),
            dma((n_fs * n_tp - 1,)),
            dma((n_fs * n_tp - 1,)),
        ],
        compiler_params=pltpu.CompilerParams(
            collective_id=0, has_side_effects=True, vmem_limit_bytes=24 * 2**20
        ),
        cost_estimate=pl.CostEstimate(
            flops=4 * tokens * width * 2 * rank, bytes_accessed=2**24, transcendentals=0
        ),
    )(x, cq, ck, bq, bk)
    shape = jax.ShapeDtypeStruct
    bf16 = jnp.bfloat16
    return pl.pallas_call(
        functools.partial(update_kernel, 2.0 * rows * n_fs * rank),
        out_shape=(
            shape(qw.shape, f32),
            shape(kw.shape, f32),
            shape(qw.shape, f32),
            shape(kw.shape, f32),
            shape(qw.shape, bf16),
            shape(kw.shape, bf16),
            shape(mean.shape, f32),
            shape(sq.shape, f32),
        ),
        compiler_params=pltpu.CompilerParams(vmem_limit_bytes=24 * 2**20),
    )(sums, total, qw, kw, bq, bk, mean, sq)


def plain(x, cq, ck, qw, kw, bq, bk, mean, sq):
    highest = lax.Precision.HIGHEST
    contract = (((0,), (0,)), ((), ()))
    f32 = jnp.float32
    bq, bk = bq.astype(f32), bk.astype(f32)
    rows, rank = qw.shape[0], bq.shape[1]
    parts = []
    for cot, basis in ((cq, bq), (ck, bk)):
        gradient = lax.dot_general(x, cot, contract, preferred_element_type=f32)
        parts.append(jnp.dot(gradient, basis, precision=lax.Precision.HIGH))
    summed = lax.psum_scatter(
        jnp.concatenate(parts, axis=1), "fs", scatter_dimension=0, tiled=True
    )
    projected = lax.psum(jnp.stack([summed[:, :rank], summed[:, rank:]]), "tp")
    total = lax.psum(jnp.sum(projected * projected), "fs")
    count = 2.0 * rows * lax.axis_size("fs") * rank
    normalized = projected * lax.rsqrt(total / count + EPSILON)
    mean = BETA_MEAN * mean + (1.0 - BETA_MEAN) * normalized
    sq = BETA_SQUARE * sq + (1.0 - BETA_SQUARE) * normalized * normalized
    direction = mean / jnp.sqrt(sq)
    query_step = lax.dot_general(direction[0], bq, NT, precision=highest)
    key_step = lax.dot_general(direction[1], bk, NT, precision=highest)
    query_new = qw - STEP_RATE * query_step
    key_new = kw - STEP_RATE * key_step
    return (
        query_step,
        key_step,
        query_new,
        key_new,
        query_new.astype(jnp.bfloat16),
        key_new.astype(jnp.bfloat16),
        mean,
        sq,
    )


def solution(mesh):
    n_fs, n_tp = mesh.shape["fs"], mesh.shape["tp"]

    def local(x, cq, ck, qw, kw, bq, bk, mean, sq):
        rows, rank = qw.shape[0], bq.shape[1]
        fits = (
            n_fs % 2 == 0
            and n_tp % 2 == 0
            and n_fs > 2
            and n_tp > 2
            and rows % 128 == 0
            and rank % (n_tp // 2 * CHUNKS * 8) == 0
        )
        if fits:
            return fast(n_fs, n_tp, x, cq, ck, qw, kw, bq, bk, mean, sq)
        return plain(x, cq, ck, qw, kw, bq, bk, mean, sq)

    in_specs = (
        P("fs", None),
        P("fs", "tp"),
        P("fs", "tp"),
        P("fs", "tp"),
        P("fs", "tp"),
        P("tp", None),
        P("tp", None),
        P(None, "fs", None),
        P(None, "fs", None),
    )
    out_specs = (
        P("fs", "tp"),
        P("fs", "tp"),
        P("fs", "tp"),
        P("fs", "tp"),
        P("fs", "tp"),
        P("fs", "tp"),
        P(None, "fs", None),
        P(None, "fs", None),
    )
    return jax.shard_map(local, mesh=mesh, in_specs=in_specs, out_specs=out_specs, check_vma=False)
```

time: 159 us -> 42.3 us (0.27)
  waiting for transfers between devices: 104 us -> 0 us
  Pallas kernels: 0 us -> 35.4 us
  blocking collectives: 22 us -> 0 us
  between operations: 14.9 us -> 0.72 us
  matrix products: 8.46 us -> 0 us
  other arithmetic: 4.88 us -> 0 us
  local copies, waits for them, and re-layouts: 3.93 us -> 5.86 us
    reduce_scatter x1 -> x0, waiting for transfers between devices: 72 us -> none  [local(): lax.psum_scatter(jnp.concatenate([jnp.dot(query_part, query_float, precis...]
    pallas_call x0 -> x2, Pallas kernels: none -> 35.4 us  [the longest x1 33.9 us: fast(): pl.pallas_call(functools.partial(reduce_kernel, n_fs, n_tp), out_shape=(j...]
    psum x1 -> x0, waiting for transfers between devices: 32.4 us -> none  [local(): projected = lax.psum(jnp.stack([query_projected, key_projected]), 'tp')]
    psum x1 -> x0, blocking collectives: 22 us -> none  [local(): total_square = lax.psum(jnp.sum(projected * projected), 'fs')]
    dot_general x6 -> x0, matrix products: 8.46 us -> none  [the longest x1 3.68 us: local(): lax.dot_general(normed_input, query_cotangent, contract, preferred_elemen...]
    unnamed x22 -> x18, local copies, waits for them, and re-layouts: 2.95 us -> 5.86 us
    reduce_sum x1 -> x0, other arithmetic: 1.62 us -> none  [local(): total_square = lax.psum(jnp.sum(projected * projected), 'fs')]
  transfers between devices with their start and end apart: 2 -> 0, of which waited for: 2 -> 0; matrix products, arithmetic and copies ran while one was open for 0% -> 0% of each run, Pallas kernels for 0% -> 0%
where the time goes in v1:
time: 42.3 us; the launch traced here: 42 us
  Pallas kernels  35.4 us (84%)
  local copies, waits for them, and re-layouts  5.86 us (14%)
  between operations  0.72 us (2%)
    pallas_call x1, Pallas kernels, fast(): pl.pallas_call(functools.partial(reduce_kernel, n_fs, n_tp), out_shape=(j...  33.9 us
    unnamed x18, local copies, waits for them, and re-layouts  5.86 us
    pallas_call x1, Pallas kernels, fast(): pl.pallas_call(functools.partial(update_kernel, 2.0 * rows * n_fs * rank)...  1.49 us

profile of v1, /device:TPU:0, one launch (start us, length us, event | category | flops | bytes accessed | tf_op | source)
XLA Modules:
  0.0 42.0 jit_solution(15686685990577925040)
XLA Ops:
  0.6 0.0 copy-start.2
  0.6 0.0 copy-start.1
  0.7 0.0 copy-start.3
  0.7 0.0 copy-start
  0.7 0.0 copy-start.4
  0.7 0.9 %copy-done.4 = bf16[256,128]{1,0:T(8,128)(2,1)S(1)} copy-done((bf16[256,128]{1,0:T(8,128)(2,1)S(1)}, bf16[256,128]{1,0:T(8,128)(2,1)}, u32[]{:S(2)}) %copy-start.4) | copy-done | bytes 65560
  1.6 0.0 copy-start.5
  1.6 0.8 %copy-done.5 = bf16[128,128]{1,0:T(8,128)(2,1)S(1)} copy-done((bf16[128,128]{1,0:T(8,128)(2,1)S(1)}, bf16[128,128]{1,0:T(8,128)(2,1)}, u32[]{:S(2)}) %copy-start.5) | copy-done | bytes 32792
  2.3 0.0 copy-start.6
  2.4 2.2 %copy-done.6 = bf16[1024,2048]{1,0:T(8,128)(2,1)S(1)} copy-done((bf16[1024,2048]{1,0:T(8,128)(2,1)S(1)}, bf16[1024,2048]{1,0:T(8,128)(2,1)}, u32[]{:S(2)}) %copy-start.6) | copy-done | bytes 4194328
  4.5 0.0 copy-start.7
  4.5 1.0 %copy-done.7 = bf16[1024,256]{1,0:T(8,128)(2,1)S(1)} copy-done((bf16[1024,256]{1,0:T(8,128)(2,1)S(1)}, bf16[1024,256]{1,0:T(8,128)(2,1)}, u32[]{:S(2)}) %copy-start.7) | copy-done | bytes 524312
  5.6 0.0 copy-start.8
  5.6 0.9 %copy-done.8 = bf16[1024,128]{1,0:T(8,128)(2,1)S(1)} copy-done((bf16[1024,128]{1,0:T(8,128)(2,1)S(1)}, bf16[1024,128]{1,0:T(8,128)(2,1)}, u32[]{:S(2)}) %copy-start.8) | copy-done | bytes 262168
  6.5 33.9 %shard_map.152 = (f32[256,256]{1,0:T(8,128)S(1)}, f32[8,128]{1,0:T(8,128)S(1)}) custom-call(bf16[1024,2048]{1,0:T(8,128)(2,1)S(1)} %copy-done.6, bf16[1024,256]{1,0:T(8,128)(2,1)S(1)} %copy-done.7, bf16[1024,128]{1,0:T(8,128)(2,1)S(1)} %copy-done.8, bf16[256,128]{1,0:T(8,128)(2,1)S(1)} %copy-done.4, bf16[128,128]{1,0:T(8,128)(2,1)S(1)} %copy-done.5), custom_call_target="tpu_custom_call" | custom-call | flops 2147483648 | bytes 16777216 | tf_op jit(solution)/shard_map/pallas_call | solution.py:282
  40.5 0.0 copy-done.2
  40.5 0.0 copy-done.1
  40.5 0.0 copy-done.3
  40.5 0.0 copy-done
  40.5 1.5 %shard_map.153 = (f32[256,256]{1,0:T(8,128)}, f32[256,128]{1,0:T(8,128)}, f32[256,256]{1,0:T(8,128)}, f32[256,128]{1,0:T(8,128)}, bf16[256,256]{1,0:T(8,128)(2,1...) custom-call(f32[256,256]{1,0:T(8,128)S(1)} %get-tuple-element.10.sums_ref, ...), custom_call_target="tpu_custom_call" | custom-call | tf_op jit(solution)/shard_map/pallas_call | solution.py:328
Async XLA Ops:
  0.6 39.8 %copy-start.2 = (f32[2,256,128]{2,1,0:T(8,128)S(1)}, f32[2,256,128]{2,1,0:T(8,128)}, u32[]{:S(2)}) copy-start(f32[2,256,128]{2,1,0:T(8,128)} %sq_ref.1) | copy-start | bytes 786436
  0.6 39.8 %copy-start.1 = (f32[2,256,128]{2,1,0:T(8,128)S(1)}, f32[2,256,128]{2,1,0:T(8,128)}, u32[]{:S(2)}) copy-start(f32[2,256,128]{2,1,0:T(8,128)} %mean_ref.1) | copy-start | bytes 786436
  0.7 39.8 %copy-start.3 = (f32[256,128]{1,0:T(8,128)S(1)}, f32[256,128]{1,0:T(8,128)}, u32[]{:S(2)}) copy-start(f32[256,128]{1,0:T(8,128)} %kw_ref.1) | copy-start | bytes 393220
  0.7 39.8 %copy-start = (f32[256,256]{1,0:T(8,128)S(1)}, f32[256,256]{1,0:T(8,128)}, u32[]{:S(2)}) copy-start(f32[256,256]{1,0:T(8,128)} %qw_ref.1) | copy-start | bytes 786436
  0.7 0.9 %copy-start.4 = (bf16[256,128]{1,0:T(8,128)(2,1)S(1)}, bf16[256,128]{1,0:T(8,128)(2,1)}, u32[]{:S(2)}) copy-start(bf16[256,128]{1,0:T(8,128)(2,1)} %bq_ref.3) | copy-start | bytes 196612
  1.6 0.8 %copy-start.5 = (bf16[128,128]{1,0:T(8,128)(2,1)S(1)}, bf16[128,128]{1,0:T(8,128)(2,1)}, u32[]{:S(2)}) copy-start(bf16[128,128]{1,0:T(8,128)(2,1)} %bk_ref.3) | copy-start | bytes 98308
  2.3 2.2 %copy-start.6 = (bf16[1024,2048]{1,0:T(8,128)(2,1)S(1)}, bf16[1024,2048]{1,0:T(8,128)(2,1)}, u32[]{:S(2)}) copy-start(bf16[1024,2048]{1,0:T(8,128)(2,1)} %x_hbm.1) | copy-start | bytes 12582916
  4.5 1.0 %copy-start.7 = (bf16[1024,256]{1,0:T(8,128)(2,1)S(1)}, bf16[1024,256]{1,0:T(8,128)(2,1)}, u32[]{:S(2)}) copy-start(bf16[1024,256]{1,0:T(8,128)(2,1)} %cq_hbm.1) | copy-start | bytes 1572868
  5.6 0.9 %copy-start.8 = (bf16[1024,128]{1,0:T(8,128)(2,1)S(1)}, bf16[1024,128]{1,0:T(8,128)(2,1)}, u32[]{:S(2)}) copy-start(bf16[1024,128]{1,0:T(8,128)(2,1)} %ck_hbm.1) | copy-start | bytes 786436

commit v2 on v1

--- a/solution.py
+++ b/solution.py
@@ -11,7 +11,7 @@
 BETA_SQUARE = 0.8
 STEP_RATE = 0.25
 EPSILON = 1e-06
-CHUNKS = 4
+CHUNKS = 2
 MESH = pl.DeviceIdType.MESH
 NT = (((1,), (1,)), ((), ()))
 
@@ -28,13 +28,15 @@
     x_hbm,
     cq_hbm,
     ck_hbm,
-    bq_ref,
-    bk_ref,
+    bq_hbm,
+    bk_hbm,
     out_ref,
     total_ref,
     x_ref,
     cq_ref,
     ck_ref,
+    bq_ref,
+    bk_ref,
     ybuf,
     ycore,
     ysum,
@@ -74,20 +76,27 @@
 
     others = [(df, dt) for df in range(n_fs) for dt in range(n_tp) if df or dt]
 
+    pairs = (
+        (bq_hbm, bq_ref),
+        (cq_hbm, cq_ref),
+        (bk_hbm, bk_ref),
+        (ck_hbm, ck_ref),
+        (x_hbm, x_ref),
+    )
     loads = [
-        pltpu.make_async_copy(cq_hbm, cq_ref, load_sem.at[0]),
-        pltpu.make_async_copy(ck_hbm, ck_ref, load_sem.at[1]),
-        pltpu.make_async_copy(x_hbm, x_ref, load_sem.at[2]),
+        pltpu.make_async_copy(src, dst, load_sem.at[i])
+        for i, (src, dst) in enumerate(pairs)
     ]
+    barrier = pltpu.get_barrier_semaphore()
+    for df, dt in reversed(others):
+        pl.semaphore_signal(barrier, inc=1, device_id=peer(df, dt), device_id_type=MESH)
     for load in loads:
         load.start()
-    barrier = pltpu.get_barrier_semaphore()
-    for df, dt in others:
-        pl.semaphore_signal(barrier, inc=1, device_id=peer(df, dt), device_id_type=MESH)
 
     per = chunks * depth
     for which, (basis, cot) in enumerate(((bq_ref, cq_ref), (bk_ref, ck_ref))):
-        loads[which].wait()
+        loads[2 * which].wait()
+        loads[2 * which + 1].wait()
         part = lax.dot_general(
             basis[...].T, cot[...], NT, preferred_element_type=jnp.float32
         )
@@ -117,6 +126,7 @@
 
     y_copies = {}
     x_copies = {}
+    order = sorted(range(1, fs_outer), key=lambda j: abs(2 * j - fs_outer)) + [0]
     z_copies = {}
     g_copies = {}
 
@@ -141,7 +151,7 @@
             value = value + yrecv[c, d - 1]
         both = jnp.concatenate(split(value), axis=0)
         if c == 0:
-            loads[2].wait()
+            loads[4].wait()
         for o in range(fs_outer):
             wide = jnp.dot(
                 both, x_ref[:, o * 2 * rows : (o + 1) * 2 * rows],
@@ -150,30 +160,32 @@
             wide = wide[:depth] + wide[depth:]
             pbuf[c, 0, o] = wide[:, :rows]
             pbuf[c, 1, o] = wide[:, rows:]
-        copy = remote(
-            pbuf.at[c, 1 - x], xrecv.at[c], x_send.at[c], x_recv.at[c],
-            (z * 2 + 1 - x, t),
-        )
-        copy.start()
-        x_copies[c] = copy
-        started.append(copy)
-
-    def stage_x(c):
-        x_copies[c].wait_recv()
-        for o in range(fs_outer):
-            qbuf[c, o] = pbuf[c, x, o] + xrecv[c, o]
-        for d in range(1, fs_outer):
-            to = lax.rem(z + d, fs_outer)
+        for j in order:
             copy = remote(
-                qbuf.at[c, to], zrecv.at[c, d - 1],
-                z_send.at[c, d - 1], z_recv.at[c, d - 1], (to * 2 + x, t),
+                pbuf.at[c, 1 - x, lax.rem(z + j, fs_outer)], xrecv.at[c, j],
+                x_send.at[c, j], x_recv.at[c, j], (z * 2 + 1 - x, t),
             )
             copy.start()
-            z_copies[c, d] = copy
+            x_copies[c, j] = copy
             started.append(copy)
 
+    def stage_x(c):
+        for j in order:
+            to = lax.rem(z + j, fs_outer)
+            x_copies[c, j].wait_recv()
+            qbuf[c, j] = pbuf[c, x, to] + xrecv[c, j]
+            if j == 0:
+                continue
+            copy = remote(
+                qbuf.at[c, j], zrecv.at[c, j - 1],
+                z_send.at[c, j - 1], z_recv.at[c, j - 1], (to * 2 + x, t),
+            )
+            copy.start()
+            z_copies[c, j] = copy
+            started.append(copy)
+
     def stage_z(c):
-        value = qbuf[c, z]
+        value = qbuf[c, 0]
         for d in range(1, fs_outer):
             z_copies[c, d].wait_recv()
             value = value + zrecv[c, d - 1]
@@ -206,6 +218,7 @@
             piece = stage_z(step - 2)
             acc = piece if acc is None else acc + piece
 
+    acc = jnp.sum(acc, axis=0, keepdims=True)
     square[...] = acc
     s_copies = []
     for i, (df, dt) in enumerate(others):
@@ -283,14 +296,16 @@
         functools.partial(reduce_kernel, n_fs, n_tp),
         out_shape=(
             jax.ShapeDtypeStruct((2 * rank, rows), f32),
-            jax.ShapeDtypeStruct((8, 128), f32),
+            jax.ShapeDtypeStruct((1, 128), f32),
         ),
-        in_specs=[hbm, hbm, hbm, vmem, vmem],
+        in_specs=[hbm] * 5,
         out_specs=(vmem, vmem),
         scratch_shapes=[
             pltpu.VMEM(x.shape, x.dtype),
             pltpu.VMEM(cq.shape, cq.dtype),
             pltpu.VMEM(ck.shape, ck.dtype),
+            pltpu.VMEM(bq.shape, bq.dtype),
+            pltpu.VMEM(bk.shape, bk.dtype),
             pltpu.VMEM((k, 2, tp_outer, depth, tokens), f32),
             pltpu.VMEM((k, tp_outer, depth, tokens), f32),
             pltpu.VMEM((k, tp_outer, depth, tokens), f32),
@@ -300,15 +315,15 @@
             pltpu.VMEM((k, fs_outer, depth, rows), f32),
             pltpu.VMEM((k, fs_outer - 1, depth, rows), f32),
             pltpu.VMEM((n_tp, k, depth, rows), f32),
-            pltpu.VMEM((8, 128), f32),
-            pltpu.VMEM((n_fs * n_tp - 1, 8, 128), f32),
-            dma((3,)),
+            pltpu.VMEM((1, 128), f32),
+            pltpu.VMEM((n_fs * n_tp - 1, 1, 128), f32),
+            dma((5,)),
             dma((k,)),
             dma((k,)),
             dma((k, tp_outer - 1)),
             dma((k, tp_outer - 1)),
-            dma((k,)),
-            dma((k,)),
+            dma((k, fs_outer)),
+            dma((k, fs_outer)),
             dma((k, fs_outer - 1)),
             dma((k, fs_outer - 1)),
             dma((k, n_tp - 1)),
@@ -317,7 +332,7 @@
             dma((n_fs * n_tp - 1,)),
         ],
         compiler_params=pltpu.CompilerParams(
-            collective_id=0, has_side_effects=True, vmem_limit_bytes=24 * 2**20
+            collective_id=0, has_side_effects=True, vmem_limit_bytes=60 * 2**20
         ),
         cost_estimate=pl.CostEstimate(
             flops=4 * tokens * width * 2 * rank, bytes_accessed=2**24, transcendentals=0

time: 42.3 us -> 35.5 us (0.84)
  local copies, waits for them, and re-layouts: 5.86 us -> 1.58 us
  Pallas kernels: 35.4 us -> 33 us
    unnamed x18 -> x16, local copies, waits for them, and re-layouts: 5.86 us -> 1.58 us
    pallas_call x1, Pallas kernels: 33.9 us -> 31.5 us  [fast(): pl.pallas_call(functools.partial(reduce_kernel, n_fs, n_tp), out_shape=(j...]
where the time goes in v2:
time: 35.5 us; the launch traced here: 35.3 us
  Pallas kernels  33 us (93%)
  local copies, waits for them, and re-layouts  1.58 us (4%)
  between operations  0.75 us (2%)
    pallas_call x1, Pallas kernels, fast(): pl.pallas_call(functools.partial(reduce_kernel, n_fs, n_tp), out_shape=(j...  31.5 us
    unnamed x16, local copies, waits for them, and re-layouts  1.58 us
    pallas_call x1, Pallas kernels, fast(): pl.pallas_call(functools.partial(update_kernel, 2.0 * rows * n_fs * rank)...  1.48 us

profile of v2, /device:TPU:0, one launch (start us, length us, event | category | flops | bytes accessed | tf_op | source)
XLA Modules:
  0.0 35.3 jit_solution(15332663449475276704)
XLA Ops:
  0.6 0.0 copy-start.6
  0.6 0.0 copy-start.5
  0.7 0.0 copy-start.2
  0.7 0.0 copy-start.1
  0.7 0.0 copy-start.4
  0.7 0.0 copy-start
  0.7 31.5 %shard_map.152 = (f32[256,256]{1,0:T(8,128)}, f32[1,128]{1,0:T(1,128)}) custom-call(bf16[1024,2048]{1,0:T(8,128)(2,1)} %x_hbm.1, bf16[1024,256]{1,0:T(8,128)(2,1)} %cq_hbm.1, bf16[1024,128]{1,0:T(8,128)(2,1)} %ck_hbm.1, bf16[256,128]{1,0:T(8,128)(2,1)} %bq_ref.1, bf16[128,128]{1,0:T(8,128)(2,1)} %bk_ref.1), custom_call_target="tpu_custom_call" | custom-call | flops 2147483648 | bytes 16777216 | tf_op jit(solution)/shard_map/pallas_call | solution.py:295
  32.2 0.0 copy-done.6
  32.2 0.0 copy-done.5
  32.2 0.0 copy-done.2
  32.2 0.0 copy-done.1
  32.2 0.0 copy-done.4
  32.3 0.0 copy-done
  32.3 0.0 copy-start.3
  32.3 0.9 %copy-done.3 = f32[256,256]{1,0:T(8,128)S(1)} copy-done((f32[256,256]{1,0:T(8,128)S(1)}, f32[256,256]{1,0:T(8,128)}, u32[]{:S(2)}) %copy-start.3) | copy-done | bytes 262168
  33.2 0.0 copy-start.7
  33.2 0.6 %copy-done.7 = f32[1,128]{1,0:T(1,128)S(1)} copy-done((f32[1,128]{1,0:T(1,128)S(1)}, f32[1,128]{1,0:T(1,128)}, u32[]{:S(2)}) %copy-start.7) | copy-done | bytes 536
  33.8 1.5 %shard_map.153 = (f32[256,256]{1,0:T(8,128)}, f32[256,128]{1,0:T(8,128)}, f32[256,256]{1,0:T(8,128)}, f32[256,128]{1,0:T(8,128)}, bf16[256,256]{1,0:T(8,128)(2,1...) custom-call(f32[256,256]{1,0:T(8,128)S(1)} %copy-done.3, f32[1,128]{1,0:T(1,128)S(1)} %copy-done.7, ...), custom_call_target="tpu_custom_call" | custom-call | tf_op jit(solution)/shard_map/pallas_call | solution.py:343
Async XLA Ops:
  0.6 31.6 %copy-start.6 = (bf16[128,128]{1,0:T(8,128)(2,1)S(1)}, bf16[128,128]{1,0:T(8,128)(2,1)}, u32[]{:S(2)}) copy-start(bf16[128,128]{1,0:T(8,128)(2,1)} %bk_ref.1) | copy-start | bytes 98308
  0.6 31.6 %copy-start.5 = (bf16[256,128]{1,0:T(8,128)(2,1)S(1)}, bf16[256,128]{1,0:T(8,128)(2,1)}, u32[]{:S(2)}) copy-start(bf16[256,128]{1,0:T(8,128)(2,1)} %bq_ref.1) | copy-start | bytes 196612
  0.7 31.6 %copy-start.2 = (f32[2,256,128]{2,1,0:T(8,128)S(1)}, f32[2,256,128]{2,1,0:T(8,128)}, u32[]{:S(2)}) copy-start(f32[2,256,128]{2,1,0:T(8,128)} %sq_ref.1) | copy-start | bytes 786436
  0.7 31.6 %copy-start.1 = (f32[2,256,128]{2,1,0:T(8,128)S(1)}, f32[2,256,128]{2,1,0:T(8,128)}, u32[]{:S(2)}) copy-start(f32[2,256,128]{2,1,0:T(8,128)} %mean_ref.1) | copy-start | bytes 786436
  0.7 31.6 %copy-start.4 = (f32[256,128]{1,0:T(8,128)S(1)}, f32[256,128]{1,0:T(8,128)}, u32[]{:S(2)}) copy-start(f32[256,128]{1,0:T(8,128)} %kw_ref.1) | copy-start | bytes 393220
  0.7 31.6 %copy-start = (f32[256,256]{1,0:T(8,128)S(1)}, f32[256,256]{1,0:T(8,128)}, u32[]{:S(2)}) copy-start(f32[256,256]{1,0:T(8,128)} %qw_ref.1) | copy-start | bytes 786436
  32.3 1.0 %copy-start.3 = (f32[256,256]{1,0:T(8,128)S(1)}, f32[256,256]{1,0:T(8,128)}, u32[]{:S(2)}) copy-start(f32[256,256]{1,0:T(8,128)} %get-tuple-element.10.sums_ref) | copy-start | bytes 786436
  33.2 0.6 %copy-start.7 = (f32[1,128]{1,0:T(1,128)S(1)}, f32[1,128]{1,0:T(1,128)}, u32[]{:S(2)}) copy-start(f32[1,128]{1,0:T(1,128)} %get-tuple-element.11.total_ref) | copy-start | bytes 1540

commit v3 on v2

--- a/solution.py
+++ b/solution.py
@@ -295,8 +295,8 @@
     sums, total = pl.pallas_call(
         functools.partial(reduce_kernel, n_fs, n_tp),
         out_shape=(
-            jax.ShapeDtypeStruct((2 * rank, rows), f32),
-            jax.ShapeDtypeStruct((1, 128), f32),
+            pltpu.VMEM((2 * rank, rows), f32),
+            pltpu.VMEM((1, 128), f32),
         ),
         in_specs=[hbm] * 5,
         out_specs=(vmem, vmem),

time: 35.5 us -> 33.2 us (0.935)
  local copies, waits for them, and re-layouts: 1.58 us -> 0.03 us
  Pallas kernels: 33 us -> 32.3 us
    unnamed x16 -> x12, local copies, waits for them, and re-layouts: 1.58 us -> 0.03 us
    pallas_call x1, Pallas kernels: 31.5 us -> 30.8 us  [fast(): pl.pallas_call(functools.partial(reduce_kernel, n_fs, n_tp), out_shape=(p...]
where the time goes in v3:
time: 33.2 us; the launch traced here: 33.1 us
  Pallas kernels  32.3 us (97%)
  between operations  0.74 us (2%)
    pallas_call x1, Pallas kernels, fast(): pl.pallas_call(functools.partial(reduce_kernel, n_fs, n_tp), out_shape=(p...  30.8 us
    pallas_call x1, Pallas kernels, fast(): pl.pallas_call(functools.partial(update_kernel, 2.0 * rows * n_fs * rank)...  1.49 us

profile of v3, /device:TPU:0, one launch (start us, length us, event | category | flops | bytes accessed | tf_op | source)
XLA Modules:
  0.0 33.1 jit_solution(16875096956407001000)
XLA Ops:
  0.6 0.0 copy-start.5
  0.6 0.0 copy-start.4
  0.7 0.0 copy-start.2
  0.7 0.0 copy-start.1
  0.7 0.0 copy-start.3
  0.7 0.0 copy-start
  0.7 30.8 %shard_map.152 = (f32[256,256]{1,0:T(8,128)S(1)}, f32[1,128]{1,0:T(1,128)S(1)}) custom-call(bf16[1024,2048]{1,0:T(8,128)(2,1)} %x_hbm.1, bf16[1024,256]{1,0:T(8,128)(2,1)} %cq_hbm.1, bf16[1024,128]{1,0:T(8,128)(2,1)} %ck_hbm.1, bf16[256,128]{1,0:T(8,128)(2,1)} %bq_ref.1, bf16[128,128]{1,0:T(8,128)(2,1)} %bk_ref.1), custom_call_target="tpu_custom_call" | custom-call | flops 2147483648 | bytes 16777216 | tf_op jit(solution)/shard_map/pallas_call | solution.py:295
  31.5 0.0 copy-done.5
  31.5 0.0 copy-done.4
  31.5 0.0 copy-done.2
  31.5 0.0 copy-done.1
  31.5 0.0 copy-done.3
  31.6 0.0 copy-done
  31.6 1.5 %shard_map.153 = (f32[256,256]{1,0:T(8,128)}, f32[256,128]{1,0:T(8,128)}, f32[256,256]{1,0:T(8,128)}, f32[256,128]{1,0:T(8,128)}, bf16[256,256]{1,0:T(8,128)(2,1...) custom-call(f32[256,256]{1,0:T(8,128)S(1)} %get-tuple-element.10.sums_ref, ...), custom_call_target="tpu_custom_call" | custom-call | tf_op jit(solution)/shard_map/pallas_call | solution.py:343
Async XLA Ops:
  0.6 30.9 %copy-start.5 = (bf16[128,128]{1,0:T(8,128)(2,1)S(1)}, bf16[128,128]{1,0:T(8,128)(2,1)}, u32[]{:S(2)}) copy-start(bf16[128,128]{1,0:T(8,128)(2,1)} %bk_ref.1) | copy-start | bytes 98308
  0.6 30.9 %copy-start.4 = (bf16[256,128]{1,0:T(8,128)(2,1)S(1)}, bf16[256,128]{1,0:T(8,128)(2,1)}, u32[]{:S(2)}) copy-start(bf16[256,128]{1,0:T(8,128)(2,1)} %bq_ref.1) | copy-start | bytes 196612
  0.7 30.9 %copy-start.2 = (f32[2,256,128]{2,1,0:T(8,128)S(1)}, f32[2,256,128]{2,1,0:T(8,128)}, u32[]{:S(2)}) copy-start(f32[2,256,128]{2,1,0:T(8,128)} %sq_ref.1) | copy-start | bytes 786436
  0.7 30.9 %copy-start.1 = (f32[2,256,128]{2,1,0:T(8,128)S(1)}, f32[2,256,128]{2,1,0:T(8,128)}, u32[]{:S(2)}) copy-start(f32[2,256,128]{2,1,0:T(8,128)} %mean_ref.1) | copy-start | bytes 786436
  0.7 30.9 %copy-start.3 = (f32[256,128]{1,0:T(8,128)S(1)}, f32[256,128]{1,0:T(8,128)}, u32[]{:S(2)}) copy-start(f32[256,128]{1,0:T(8,128)} %kw_ref.1) | copy-start | bytes 393220
  0.7 30.9 %copy-start = (f32[256,256]{1,0:T(8,128)S(1)}, f32[256,256]{1,0:T(8,128)}, u32[]{:S(2)}) copy-start(f32[256,256]{1,0:T(8,128)} %qw_ref.1) | copy-start | bytes 786436
